TPU v7x, 32 devices: a whole 2x2x4 slice. The times are simulated.
32 devices in a mesh: sp: 8 (over z, x), tp: 4 (over y, core).
Axes of the slice: x: 2, y: 2, z: 4, core: 2. Of those that a mesh axis runs over, the one named last changes fastest.
Arguments:
- resid: bfloat16 [4096, 2048], P(('sp', 'tp')), may hold values from -6 to 6
- pool_in: bfloat16 [4096, 1024], P('sp', 'tp'), may hold values from -8 to 8
- doc_ids: int32 [4096], P('sp'), may hold values from 0 to 3, never falling along the last dimension, each value on 1 to 1536 neighbouring positions
- w_group: bfloat16 [8, 128, 128], replicated, may hold values from -0.5 to 0.5
- pool_scale: bfloat16 [1024], replicated, may hold values from 0.099609375 to 1.8984375
- w_branch: bfloat16 [1024, 2048], P('tp'), may hold values from -0.1875 to 0.1875
- norm_gain: bfloat16 [2048], replicated, may hold values from 0.099609375 to 1.8984375
- route_ids: int32 [4096, 4], P(('sp', 'tp')), may hold values from 0 to 31, all different within a row; in each aligned block of 128 rows (0 to 127, 128 to 255, ...) at most 32 rows name the same one
- route_wts: float32 [4096, 4], P(('sp', 'tp')), may hold values from 0.2 to 1
- w_exp_gate: bfloat16 [32, 2048, 512], P(('sp', 'tp')), may hold values from -0.125 to 0.125
- w_exp_up: bfloat16 [32, 2048, 512], P(('sp', 'tp')), may hold values from -0.125 to 0.125
- w_exp_down: bfloat16 [32, 512, 2048], P(('sp', 'tp')), may hold values from -0.25 to 0.25
- w_sh_gate: bfloat16 [2048, 512], replicated, may hold values from -0.125 to 0.125
- w_sh_up: bfloat16 [2048, 512], replicated, may hold values from -0.125 to 0.125
- w_sh_down: bfloat16 [512, 2048], replicated, may hold values from -0.25 to 0.25
- final_gain: bfloat16 [2048], replicated, may hold values from 0.099609375 to 1.8984375
Outputs:
- final: bfloat16 [4096, 2048], P(('sp', 'tp'))
Inputs may be any that keep to these rules, and one draw needn't show every extreme that they name: `doc_ids`: never falls along the positions. `route_ids`: each row names 4 different experts; among the rows of one device (aligned blocks of 128 rows) no expert is named by more than 32 rows, a bound that some block reaches.
All inputs are finite; a program needn't handle non-finite values.
Results may differ from a plain program's by a relative error of at most 0.0062.
Values may be sent and summed in bfloat16 or wider, within the bound.
A program may use at most 128 MiB of HBM per device.

v0:
```python
import jax
import jax.numpy as jnp
from jax import lax
from jax.sharding import PartitionSpec as P

pool_windows = (2, 4, 8, 16, 16, 32, 64, 128)
alpha_mix = 8.0**0.25
norm_eps = 1e-05


def carried_in(value, axis, combine, identity):
    length, here = (lax.axis_size(axis), lax.axis_index(axis))
    everything = jax.tree.map(lambda part: lax.all_gather(part, axis), value)
    start = jax.tree.map(
        lambda part, zero: jnp.broadcast_to(jnp.asarray(zero, part.dtype), part.shape),
        value,
        identity,
    )

    def lap(k, before):
        reached = k < here
        new = combine(before, jax.tree.map(lambda part: part[k], everything))
        return jax.tree.map(lambda a, b: jnp.where(reached, a, b), new, before)

    return lax.fori_loop(0, length, lap, start)


def shifted(value, axis, by):
    length = lax.axis_size(axis)
    pairs = [(i, i + by) for i in range(length) if 0 <= i + by < length]
    return lax.ppermute(value, axis, pairs)


def layer_norm(values, scales):
    center = values - jnp.mean(values, axis=-1, keepdims=True)
    spread = jnp.mean(center * center, axis=-1, keepdims=True)
    return center * lax.rsqrt(spread + norm_eps) * scales.astype(jnp.float32)


def channel_windows(first_channel, channel_count, group_width):
    groups = (first_channel + jnp.arange(channel_count, dtype=jnp.int32)) // group_width
    window_table = jnp.asarray(pool_windows, dtype=jnp.int32)
    matches = groups[:, None] == jnp.arange(len(pool_windows), dtype=jnp.int32)[None, :]
    return jnp.sum(jnp.where(matches, window_table[None, :], 0), axis=1).astype(jnp.float32)


def swiglu_hidden(token_rows, gate_weight, up_weight):
    gate_vals = jnp.dot(token_rows, gate_weight, preferred_element_type=jnp.float32)
    up_vals = jnp.dot(token_rows, up_weight, preferred_element_type=jnp.float32)
    return (jax.nn.silu(gate_vals) * up_vals).astype(jnp.bfloat16)


def join_prefix(earlier, later):
    early_doc, early_count, early_sums = earlier
    late_doc, late_count, late_sums = later
    is_empty = late_count == 0.0
    same_doc = late_doc == early_doc
    new_doc = jnp.where(is_empty, early_doc, late_doc)
    new_count = jnp.where(
        is_empty, early_count, jnp.where(same_doc, early_count + late_count, late_count)
    )
    new_sums = jnp.where(
        is_empty, early_sums, jnp.where(same_doc, early_sums + late_sums, late_sums)
    )
    return (new_doc, new_count, new_sums)


def local(
    resid,
    pool_in,
    doc_ids,
    w_group,
    pool_scale,
    w_branch,
    norm_gain,
    route_ids,
    route_wts,
    w_exp_gate,
    w_exp_up,
    w_exp_down,
    w_sh_gate,
    w_sh_up,
    w_sh_down,
    final_gain,
):
    tok_count, local_width = pool_in.shape
    group_width = w_group.shape[1]
    halo_rows = max(pool_windows) - 1
    channel_first = lax.axis_index("tp") * local_width
    values = pool_in.astype(jnp.float32)
    positions = jnp.arange(tok_count, dtype=jnp.int32)
    last_doc = doc_ids[-1]
    change = jnp.concatenate([jnp.ones((1,), bool), doc_ids[1:] != doc_ids[:-1]])
    doc_start = lax.cummax(jnp.where(change, positions, 0), axis=0)
    trailing = doc_ids == last_doc
    tail_sums = jnp.sum(jnp.where(trailing[:, None], values, 0.0), axis=0)
    tail_count = jnp.sum(trailing.astype(jnp.float32)).reshape(1)
    tail_doc = last_doc.astype(jnp.float32).reshape(1)
    identity = (
        jnp.full((1,), -1.0, jnp.float32),
        jnp.zeros((1,), jnp.float32),
        jnp.zeros((local_width,), jnp.float32),
    )
    prev_doc, prev_count, prev_sums = carried_in(
        (tail_doc, tail_count, tail_sums), "sp", join_prefix, identity
    )
    before = shifted(pool_in[tok_count - halo_rows :], "sp", 1)
    extended = jnp.concatenate([before, pool_in], axis=0).astype(jnp.float32)
    cumulative = jnp.concatenate(
        [jnp.zeros((1, local_width), jnp.float32), jnp.cumsum(extended, axis=0)], axis=0
    )
    current = cumulative[halo_rows + 1 :]
    local_cum = current - cumulative[halo_rows]
    local_zero = jnp.concatenate([jnp.zeros((1, local_width), jnp.float32), local_cum], axis=0)
    carried = doc_ids.astype(jnp.float32) == prev_doc
    running = (
        local_cum - local_zero[doc_start] + jnp.where(carried[:, None], prev_sums[None, :], 0.0)
    )
    since_start = (positions - doc_start).astype(jnp.float32) + jnp.where(carried, prev_count, 0.0)
    since_start = since_start[:, None]
    doc_mean = running / (since_start + 1.0)
    widths = channel_windows(channel_first, local_width, group_width)[None, :]
    recent = running
    for window in sorted(set(pool_windows)):
        lagged = cumulative[halo_rows + 1 - window : halo_rows + 1 - window + tok_count]
        recent = jnp.where((widths == window) & (since_start >= window), current - lagged, recent)
    window_mean = recent / jnp.minimum(since_start + 1.0, widths)
    offset = (0.5 * (window_mean + doc_mean) - values).astype(jnp.bfloat16)
    group_count = local_width // group_width
    local_groups = lax.dynamic_slice_in_dim(
        w_group, lax.axis_index("tp") * group_count, group_count, 0
    )
    mixed_rows = jnp.einsum(
        "tgc,gcd->tgd",
        offset.reshape(tok_count, group_count, group_width),
        local_groups,
        preferred_element_type=jnp.float32,
    ).reshape(tok_count, local_width)
    scale_local = lax.dynamic_slice_in_dim(pool_scale, channel_first, local_width, 0).astype(
        jnp.float32
    )
    mixed_rows = (mixed_rows * scale_local[None, :]).astype(jnp.bfloat16)
    row_count, model_width = resid.shape
    token_rows = lax.all_to_all(mixed_rows, "tp", split_axis=0, concat_axis=1, tiled=True)
    branch = jnp.dot(
        token_rows,
        lax.all_gather(w_branch, "tp", axis=0, tiled=True),
        preferred_element_type=jnp.float32,
    )
    normed = layer_norm(alpha_mix * resid.astype(jnp.float32) + branch, norm_gain).astype(
        jnp.bfloat16
    )
    top_count = route_ids.shape[1]
    expert_total = lax.axis_size("sp") * lax.axis_size("tp")
    capacity = 2 * row_count * top_count // expert_total
    flat_ids = route_ids.reshape(-1)
    onehot = (flat_ids[:, None] == jnp.arange(expert_total, dtype=jnp.int32)[None, :]).astype(
        jnp.int32
    )
    slot_rank = jnp.sum(jnp.cumsum(onehot, axis=0) * onehot, axis=1) - 1
    slot_index = flat_ids * capacity + slot_rank
    assign_total = row_count * top_count
    source = jnp.full((expert_total * capacity,), assign_total, jnp.int32)
    source = source.at[slot_index].set(jnp.arange(assign_total, dtype=jnp.int32))
    padded = jnp.concatenate([normed, jnp.zeros((1, model_width), jnp.bfloat16)], axis=0)
    outgoing = padded[source // top_count].reshape(expert_total, capacity, model_width)
    arrived = lax.all_to_all(outgoing, ("sp", "tp"), split_axis=0, concat_axis=0, tiled=True)
    flat_rows = arrived.reshape(-1, model_width)
    hidden = swiglu_hidden(flat_rows, w_exp_gate[0], w_exp_up[0])
    expert_out = jnp.dot(hidden, w_exp_down[0], preferred_element_type=jnp.float32).astype(
        jnp.bfloat16
    )
    returned = lax.all_to_all(
        expert_out.reshape(arrived.shape), ("sp", "tp"), split_axis=0, concat_axis=0, tiled=True
    )
    returned = returned.reshape(expert_total * capacity, model_width)
    picked = returned[slot_index].astype(jnp.float32).reshape(row_count, top_count, model_width)
    routed = jnp.sum(picked * route_wts[:, :, None], axis=1)
    shared = jnp.dot(
        swiglu_hidden(normed, w_sh_gate, w_sh_up), w_sh_down, preferred_element_type=jnp.float32
    )
    return layer_norm(alpha_mix * normed.astype(jnp.float32) + routed + shared, final_gain).astype(
        jnp.bfloat16
    )


def solution(mesh):
    placed = (
        P(("sp", "tp"), None),
        P("sp", "tp"),
        P("sp"),
        P(),
        P(),
        P("tp", None),
        P(),
        P(("sp", "tp"), None),
        P(("sp", "tp"), None),
        P(("sp", "tp"), None, None),
        P(("sp", "tp"), None, None),
        P(("sp", "tp"), None, None),
        P(),
        P(),
        P(),
        P(),
    )
    return jax.shard_map(
        local, mesh=mesh, in_specs=placed, out_specs=P(("sp", "tp"), None), check_vma=False
    )
```

profile of v0, /device:TPU:0, one launch (start us, length us, event | category | flops | bytes accessed | tf_op | source)
XLA Modules:
  0.0 369.8 jit_solution(11847515361209987746)
XLA Ops:
  6.6 1.0 slice.74
  7.6 4.9 %collective-permute-start = (bf16[127,256]{1,0:T(8,128)(2,1)S(1)}, bf16[127,256]{1,0:T(8,128)(2,1)S(1)}, u32[]{:S(2)}, u32[]{:S(2)}) collective-permute-start(bf16[127,256]{1,0:T(8,128)(2,1)S(1)} %slice.74), channel_id=1, source_target_pairs={{0,4},{4,8},{8,12},{12,16},{16,20},{20,24},{24,28},{1,5},{5,9},{9,... | collective-permute-start | bytes 195080 | tf_op jit(solution)/shard_map/ppermute | solution.py:31
  12.5 1.3 slice.73
  13.8 1.9 convert_reduce_fusion
  18.9 1.1 fusion.17
  20.0 18.7 %all-gather.1 = f32[8,1,256]{2,1,0:T(1,128)S(1)} all-gather(f32[1,1,256]{2,1,0:T(1,128)S(1)} %bitcast.132), channel_id=2, replica_groups=mesh['sp'=8,'tp'=4] {'sp'}, dimensions={0}, use_global_device_ids=true | all-gather | bytes 9216 | tf_op jit(solution)/shard_map/all_gather | solution.py:13
  41.2 1.2 reduce-window.29
  43.5 1.3 dynamic-update-slice
  45.6 17.1 %all-reduce.6 = (f32[8]{0:T(128)S(1)}, f32[8]{0:T(128)S(1)}) all-reduce(f32[8]{0:T(128)S(1)} %dynamic-update-slice, f32[8]{0:T(128)S(1)} %dynamic-update-slice.1), channel_id=1, replica_groups=mesh['sp'=8,'tp'=4] {'sp'}, use_global_device_ids=true, to_apply=%add.4 | all-reduce | flops 16 | bytes 128
  62.8 3.0 scatter_custom_fusion
  65.9 28.7 %while.18 = (s32[]{:T(128)}, f32[1]{0:T(128)}, f32[1]{0:T(128)}, f32[256]{0:T(256)S(1)}, s32[]{:T(128)}, /*index=5*/f32[8,1]{0,1:T(1,128)S(1)}, f32[8,1]{0,1:T(1...) while((s32[]{:T(128)}, f32[1]{0:T(128)}, f32[1]{0:T(128)}, ...), condition=%wide.region_6.7_spmd.clone, body=%wide.region_5.6_spmd.clone.sunk | while | flops 1292 | bytes 5370 | solution.py:25
  97.7 1.3 dynamic-slice_convert_fusion
  100.8 2.4 gather_fusion
  103.2 3.6 convolution_bitcast_fusion
  106.8 1.3 reshape.240
  108.1 1.5 fusion.24
  109.6 3.4 all-to-all-start
  113.0 5.9 %all-to-all-done = bf16[4,128,256]{1,2,0:T(8,128)(2,1)S(1)} async-done(((bf16[4,128,256]{1,2,0:T(8,128)(2,1)}), bf16[4,128,256]{1,2,0:T(8,128)(2,1)S(1)}, u32[]{:S(2)}, u32[]{:S(2)}) %all-to-all-start) | async-done | bytes 262176 | tf_op jit(solution)/shard_map/all_to_all | solution.py:144
  118.9 3.0 fusion.50
  122.5 6.0 %gather_fusion.1 = bf16[1024,2048]{1,0:T(8,128)(2,1)} fusion(bf16[129,2048]{1,0:T(8,128)(2,1)S(1)} %concatenate.22, s32[1024]{0:T(1024)S(1)} %fusion.40), kind=kCustom, calls=%fused_computation.1 | custom fusion | bytes 8392704 | tf_op jit(solution)/shard_map/gather | solution.py:166
  128.5 96.5 %all_to_all.26 = bf16[32,32,2048]{2,1,0:T(8,128)(2,1)S(1)} all-to-all(bf16[32,32,2048]{2,1,0:T(8,128)(2,1)} %bitcast.112), channel_id=1, replica_groups=mesh['sp'=8,'tp'=4] {'sp','tp'}, dimensions={0} | all-to-all | bytes 8388608 | tf_op jit(solution)/shard_map/all_to_all | solution.py:167
  225.1 2.0 copy-done.2
  227.0 3.7 %fusion.1 = f32[1024,512]{1,0:T(8,128)} fusion(bf16[1024,2048]{1,0:T(8,128)(2,1)S(1)} %bitcast.114, bf16[1,2048,512]{2,1,0:T(8,128)(2,1)S(1)} %copy-done.13), kind=kOutput, calls=%fused_computation.14 | convolution fusion | flops 2147483648 | bytes 8388608 | tf_op jit(solution)/shard_map/dot_general | solution.py:49
  230.8 10.1 %convolution_convert_fusion = bf16[1024,2048]{1,0:T(8,128)(2,1)} fusion(bf16[1,512,2048]{2,1,0:T(8,128)(2,1)S(1)} %copy-done, f32[1024,512]{1,0:T(8,128)} %fusion.1, bf16[1024,2048]{1,0:T(8,128)(2,1)} %bitcast.115, bf16[1,2048,512]{2,1,0:T(8,128)(2,1)} %param.28), kind=kOutput, calls=%fused_computation.10 | convolution fusion | flops 4300210176 | bytes 14680064 | tf_op jit(solution)/shard_map/dot_general | solution.py:170
  240.8 3.9 %all-to-all-start.2 = ((bf16[32,32,2048]{2,1,0:T(8,128)(2,1)}), bf16[32,32,2048]{2,1,0:T(8,128)(2,1)}, u32[]{:S(2)}, u32[]{:S(2)}) async-start(bf16[32,32,2048]{2,1,0:T(8,128)(2,1)} %bitcast.113), calls=%async_computation.2 | async-start | bytes 8388608 | tf_op jit(solution)/shard_map/all_to_all | solution.py:173
  244.9 2.0 fusion.52
  247.0 91.8 %all-to-all-done.2 = bf16[32,32,2048]{2,1,0:T(8,128)(2,1)} async-done(((bf16[32,32,2048]{2,1,0:T(8,128)(2,1)}), bf16[32,32,2048]{2,1,0:T(8,128)(2,1)}, u32[]{:S(2)}, u32[]{:S(2)}) %all-to-all-start.2) | async-done | bytes 4194336 | tf_op jit(solution)/shard_map/all_to_all | solution.py:173
  338.8 8.0 %gather_fusion.2 = bf16[512,2048]{1,0:T(8,128)(2,1)} fusion(bf16[1024,2048]{1,0:T(8,128)(2,1)} %bitcast.32, s32[1024]{0:T(1024)S(1)} %pad_clamp_fusion), kind=kCustom, calls=%fused_computation.2 | custom fusion | bytes 4196352 | tf_op jit(solution)/shard_map/gather | solution.py:177
  346.8 4.8 %reshape.247 = f32[128,4,2048]{2,1,0:T(4,128)} reshape(bf16[512,2048]{1,0:T(8,128)(2,1)} %gather_fusion.2) | data formatting | bytes 6291456 | tf_op jit(solution)/shard_map/convert_element_type | solution.py:177
  351.5 6.3 %multiply_reduce_fusion = f32[128,2048]{1,0:T(8,128)} fusion(f32[128,4,2048]{2,1,0:T(4,128)} %reshape.247, f32[128,4]{1,0:T(8,128)S(1)} %copy.51), kind=kLoop, calls=%fused_computation.9 | loop fusion | flops 1835008 | bytes 5244928 | tf_op jit(solution)/shard_map/reduce_sum | solution.py:178
  357.9 3.8 %fusion.51 = (f32[128]{0:T(128)S(1)}, f32[128,2048]{1,0:T(8,128)S(1)}) fusion(bf16[512,2048]{1,0:T(8,128)(2,1)} %param.33, bf16[128,2048]{1,0:T(8,128)(2,1)} %copy-done.1, bf16[2048,512]{1,0:T(8,128)(2,1)} %param.32, f32[128,512]{1,0:T(8,128)S(1)} %fusion.52, f32[128,2048]{1,0:T(8,128)} %multiply_reduce_fusion), kind=kOutput, calls=%fused_computation.133 | convolution fusion | flops 538574720 | bytes 7078400 | tf_op jit(solution)/shard_map/dot_general | solution.py:179
  361.9 1.0 multiply_convert_fusion.1
  (116 shorter events, 17.9 us)
Async XLA Ops:
  6.5 224.2 %copy-start = (bf16[1,512,2048]{2,1,0:T(8,128)(2,1)S(1)}, bf16[1,512,2048]{2,1,0:T(8,128)(2,1)}, u32[]{:S(2)}) copy-start(bf16[1,512,2048]{2,1,0:T(8,128)(2,1)} %param.30) | copy-start | bytes 6291460
  6.5 36.3 %copy-start.14 = (u32[32]{0:T(128)S(1)}, u32[32]{0:T(128)}, u32[]{:S(2)}) copy-start(u32[32]{0:T(128)} %constant.167) | copy-start | bytes 388
  6.5 92.5 %copy-start.3 = (bf16[512,256]{1,0:T(8,128)(2,1)S(1)}, bf16[512,256]{1,0:T(8,128)(2,1)}, u32[]{:S(2)}) copy-start(bf16[512,256]{1,0:T(8,128)(2,1)} %param.20) | copy-start | bytes 786436
  6.5 88.1 %copy-start.5 = (s32[512]{0:T(512)S(1)}, s32[512]{0:T(512)}, u32[]{:S(2)}) copy-start(s32[512]{0:T(512)} %param.21) | copy-start | bytes 6148
  6.5 112.4 %all-gather.4.cloned.1.call-start = ((), (), s32[]{:S(2)}) async-start(), calls=%async_computation.3 | async-start | bytes 5242880 | tf_op jit(solution)/shard_map/all_gather | solution.py:147
  7.6 91.4 %collective-permute-start = (bf16[127,256]{1,0:T(8,128)(2,1)S(1)}, bf16[127,256]{1,0:T(8,128)(2,1)S(1)}, u32[]{:S(2)}, u32[]{:S(2)}) collective-permute-start(bf16[127,256]{1,0:T(8,128)(2,1)S(1)} %slice.74), channel_id=1, source_target_pairs={{0,4},{4,8},{8,12},{12,16},{16,20},{20,24},{24,28},{1,5},{5,9},{9,... | collective-permute-start | bytes 195080 | tf_op jit(solution)/shard_map/ppermute | solution.py:31
  62.8 3.1 copy-start.8
  94.6 4.5 %copy-start.6 = (f32[256]{0:T(256)}, f32[256]{0:T(256)S(1)}, u32[]{:S(2)}) copy-start(f32[256]{0:T(256)S(1)} %get-tuple-element.148) | copy-start | bytes 3076
  100.2 0.5 copy-start.10
  106.8 6.2 %copy-start.7 = (s32[1024]{0:T(1024)S(1)}, s32[1024]{0:T(1024)}, u32[]{:S(2)}) copy-start(s32[1024]{0:T(1024)} %scatter_custom_fusion) | copy-start | bytes 12292
  106.8 12.1 %copy-start.4 = (bf16[128,2048]{1,0:T(8,128)(2,1)S(1)}, bf16[128,2048]{1,0:T(8,128)(2,1)}, u32[]{:S(2)}) copy-start(bf16[128,2048]{1,0:T(8,128)(2,1)} %param.19) | copy-start | bytes 1572868
  109.6 9.4 %all-to-all-start = ((bf16[4,128,256]{1,2,0:T(8,128)(2,1)}), bf16[4,128,256]{1,2,0:T(8,128)(2,1)S(1)}, u32[]{:S(2)}, u32[]{:S(2)}) async-start(bf16[4,128,256]{1,2,0:T(8,128)(2,1)} %fusion.24), calls=%async_computation | async-start | bytes 524288 | tf_op jit(solution)/shard_map/all_to_all | solution.py:144
  122.5 122.5 %copy-start.1 = (bf16[128,2048]{1,0:T(8,128)(2,1)}, bf16[128,2048]{1,0:T(8,128)(2,1)S(1)}, u32[]{:S(2)}) copy-start(bf16[128,2048]{1,0:T(8,128)(2,1)S(1)} %multiply_convert_fusion.2) | copy-start | bytes 1572868
  128.5 98.5 %copy-start.13 = (bf16[1,2048,512]{2,1,0:T(8,128)(2,1)S(1)}, bf16[1,2048,512]{2,1,0:T(8,128)(2,1)}, u32[]{:S(2)}) copy-start(bf16[1,2048,512]{2,1,0:T(8,128)(2,1)} %param.29) | copy-start | bytes 6291460
  225.1 2.0 copy-start.2
  240.8 4.0 %copy-start.12 = (f32[128,4]{0,1:T(4,128)S(1)}, f32[128,4]{0,1:T(4,128)}, u32[]{:S(2)}) copy-start(f32[128,4]{0,1:T(4,128)} %param.27) | copy-start | bytes 6148
  240.8 4.1 %copy-start.11 = (bf16[2048]{0:T(1024)(128)(2,1)S(1)}, bf16[2048]{0:T(1024)(128)(2,1)}, u32[]{:S(2)}) copy-start(bf16[2048]{0:T(1024)(128)(2,1)} %param.34) | copy-start | bytes 12292
  240.8 4.1 %copy-start.9 = (s32[512,1]{0,1:T(1,128)S(1)}, s32[512,1]{0,1:T(1,128)}, u32[]{:S(2)}) copy-start(s32[512,1]{0,1:T(1,128)} %copy-done.8) | copy-start | bytes 6148
  240.8 98.0 %all-to-all-start.2 = ((bf16[32,32,2048]{2,1,0:T(8,128)(2,1)}), bf16[32,32,2048]{2,1,0:T(8,128)(2,1)}, u32[]{:S(2)}, u32[]{:S(2)}) async-start(bf16[32,32,2048]{2,1,0:T(8,128)(2,1)} %bitcast.113), calls=%async_computation.2 | async-start | bytes 8388608 | tf_op jit(solution)/shard_map/all_to_all | solution.py:173
Sparse Core Ops, SparseCore 0:
  12.6 34.7 all-gather.3
where the time goes:
time: 371 us; the launch traced here: 370 us
  blocking collectives  132 us (36%)
  waiting for transfers between devices  97.8 us (26%)
  local copies, waits for them, and re-layouts  39.7 us (11%)
  matrix products  26.2 us (7%)
  loops' own time  23.8 us (6%)
  other arithmetic  23.3 us (6%)
  between operations  14.4 us (4%)
  starting transfers between devices  12.3 us (3%)
    all_to_all x1, blocking collectives, local(): lax.all_to_all(outgoing, ('sp', 'tp'), split_axis=0, concat_axis=0, tiled...  96.5 us
    all_to_all x1, waiting for transfers between devices, local(): lax.all_to_all(expert_out.reshape(arrived.shape), ('sp', 'tp'), split_axi...  91.8 us
    another operation x1, loops' own time, carried_in(): return lax.fori_loop(0, length, lap, start)  23.8 us
    all_gather x1, blocking collectives, carried_in(): everything = jax.tree.map(lambda part: lax.all_gather(part, axis), value)  18.7 us
    unnamed x1, blocking collectives  17.1 us
    dot_general x1, matrix products, local(): jnp.dot(hidden, w_exp_down[0], preferred_element_type=jnp.float32)  10.1 us
    gather x1, local copies, waits for them, and re-layouts, local(): returned[slot_index].astype(jnp.float32)  7.96 us
  transfers between devices with their start and end apart: 4, of which 2 were waited for; matrix products, arithmetic and copies ran while one was open for 10% of the time, Pallas kernels for 0%

commit v1 on v0

v1 whole, which is shorter than its diff:
```python
import functools

import jax
import jax.numpy as jnp
from jax import lax
from jax.experimental import pallas as pl
from jax.experimental.pallas import tpu as pltpu
from jax.sharding import PartitionSpec as P

pool_windows = (2, 4, 8, 16, 16, 32, 64, 128)
alpha_mix = 8.0**0.25
norm_eps = 1e-05
halo = max(pool_windows)
MESH = pl.DeviceIdType.MESH
wb_chunks = 4


def layer_norm(values, gain):
    center = values - jnp.mean(values, axis=-1, keepdims=True)
    spread = jnp.mean(center * center, axis=-1, keepdims=True)
    return center * lax.rsqrt(spread + norm_eps) * gain.astype(jnp.float32)


def dot(a, b):
    return jnp.dot(a, b, preferred_element_type=jnp.float32)


def silu_mul(gate, up):
    return (gate / (1.0 + jnp.exp(-gate)) * up).astype(jnp.bfloat16)


def pool_kernel(
    n_sp, n_tp,
    pool_ref, docc_ref, docr_ref, wg_ref, scale_ref, wb_ref, resid_ref, gain_ref,
    out_ref,
    ext, stats, mixed, token_rows, wb_all,
    stat_send, stat_recv, halo_send, halo_recv, mix_send, mix_recv,
    wb_send, wb_recv, fw_send, wb_local,
):
    s, p = lax.axis_index("sp"), lax.axis_index("tp")
    toks, width = pool_ref.shape
    group_width = wg_ref.shape[1]
    rows = resid_ref.shape[0]
    depth = wb_ref.shape[0]
    piece = depth // wb_chunks
    partner = p + 1 - 2 * lax.rem(p, 2)

    barrier = pltpu.get_barrier_semaphore()
    for k in range(1, n_sp):
        pl.semaphore_signal(barrier, inc=1, device_id=(lax.rem(s + k, n_sp), p), device_id_type=MESH)
    for k in range(1, n_tp):
        pl.semaphore_signal(barrier, inc=1, device_id=(s, lax.rem(p + k, n_tp)), device_id_type=MESH)
    pl.semaphore_wait(barrier, n_sp + n_tp - 2)

    def wb_copy(c, src, slot, target, send, recv):
        window = pl.ds(c * piece, piece)
        return pltpu.make_async_remote_copy(
            src_ref=src.at[window], dst_ref=wb_all.at[slot, window],
            send_sem=send, recv_sem=recv, device_id=(s, target), device_id_type=MESH,
        )

    own_wb = pltpu.make_async_copy(wb_ref, wb_all.at[p], wb_local)
    own_wb.start()

    values = pool_ref[...]
    docc, docr = docc_ref[...], docr_ref[...]
    last = jnp.max(docr, axis=1, keepdims=True)
    first = jnp.min(docr, axis=1, keepdims=True).astype(jnp.float32)
    tail = (docr == last).astype(jnp.float32)
    tail_count = jnp.sum(tail, axis=1, keepdims=True)
    sums = dot(jnp.broadcast_to(tail, (8, toks)).astype(jnp.bfloat16), values)
    lane = lax.broadcasted_iota(jnp.int32, (8, 128), 1)
    stats[s, :, 0:width] = sums
    stats[s, :, width : width + 128] = jnp.where(lane == 0, last.astype(jnp.float32), tail_count)

    halo_copy = pltpu.make_async_remote_copy(
        src_ref=pool_ref.at[pl.ds(toks - halo, halo)], dst_ref=ext.at[pl.ds(0, halo)],
        send_sem=halo_send, recv_sem=halo_recv,
        device_id=(lax.rem(s + 1, n_sp), p), device_id_type=MESH,
    )
    halo_copy.start()
    ext[halo:, :] = values

    tpos = lax.broadcasted_iota(jnp.int32, (toks, toks), 0)
    spos = lax.broadcasted_iota(jnp.int32, (toks, toks), 1)
    same = ((docc == docr) & (spos <= tpos)).astype(jnp.float32)
    here = jnp.sum(same, axis=1, keepdims=True)
    running = dot(same.astype(jnp.bfloat16), values)

    stat_copies = []
    for k in range(1, n_sp):
        stat_copies.append(
            pltpu.make_async_remote_copy(
                src_ref=stats.at[s], dst_ref=stats.at[s],
                send_sem=stat_send.at[k], recv_sem=stat_recv.at[k],
                device_id=(lax.rem(s + k, n_sp), p), device_id_type=MESH,
            )
        )
        stat_copies[-1].start()

    cross = []
    for c in range(wb_chunks):
        for j in range(1, n_tp // 2):
            cross.append(
                wb_copy(c, wb_ref, p, lax.rem(p + 2 * j, n_tp), wb_send.at[j, c], wb_recv.at[2 * j, c])
            )
            cross[-1].start()
    beside = [wb_copy(c, wb_ref, p, partner, wb_send.at[0, c], wb_recv.at[1, c]) for c in range(wb_chunks)]
    for copy in beside:
        copy.start()

    for copy in stat_copies:
        copy.wait_recv()
    prev_count = jnp.zeros((1, 1), jnp.float32)
    prev_sums = jnp.zeros((1, width), jnp.float32)
    for k in range(n_sp):
        block = stats[k]
        joined = (block[0:1, width : width + 1] == first) & (k < s)
        prev_count = prev_count + jnp.where(joined, block[0:1, width + 1 : width + 2], 0.0)
        prev_sums = prev_sums + jnp.where(joined, block[0:1, 0:width], 0.0)
    carried = docc.astype(jnp.float32) == first
    length = here + jnp.where(carried, prev_count, 0.0)
    running = running + jnp.where(carried, prev_sums, 0.0)
    doc_mean = running / length

    halo_copy.wait_recv()
    tpos = lax.broadcasted_iota(jnp.int32, (toks, toks + halo), 0) + halo
    spos = lax.broadcasted_iota(jnp.int32, (toks, toks + halo), 1)
    back = tpos - spos
    groups = width // group_width
    for i in range(groups):
        g = p * groups + i
        window = jnp.int32(0)
        for at, size in enumerate(pool_windows):
            window = jnp.where(g == at, size, window)
        span = jnp.minimum(length, window.astype(jnp.float32))
        band = ((back >= 0) & (back < span.astype(jnp.int32))).astype(jnp.float32).astype(jnp.bfloat16)
        cols = slice(i * group_width, (i + 1) * group_width)
        recent = dot(band, ext[:, cols])
        offset = 0.5 * (recent / span + doc_mean[:, cols]) - values[:, cols].astype(jnp.float32)
        turned = dot(offset.astype(jnp.bfloat16), wg_ref[g])
        scale = scale_ref[0:1, pl.ds(pl.multiple_of(g * group_width, group_width), group_width)]
        mixed[:, cols] = (turned * scale.astype(jnp.float32)).astype(jnp.bfloat16)

    mix_copies = []
    for k in range(1, n_tp):
        q = lax.rem(p + k, n_tp)
        mix_copies.append(
            pltpu.make_async_remote_copy(
                src_ref=mixed.at[pl.ds(pl.multiple_of(q * rows, rows), rows)], dst_ref=token_rows.at[p],
                send_sem=mix_send.at[k], recv_sem=mix_recv.at[k],
                device_id=(s, q), device_id_type=MESH,
            )
        )
        mix_copies[-1].start()
    token_rows[p] = mixed[pl.ds(pl.multiple_of(p * rows, rows), rows), :]

    onward = []
    for c in range(wb_chunks):
        for j in range(1, n_tp // 2):
            slot = lax.rem(p - 2 * j + n_tp, n_tp)
            cross[c * (n_tp // 2 - 1) + j - 1].wait_recv()
            onward.append(
                wb_copy(c, wb_all.at[slot], slot, partner, fw_send.at[j, c], wb_recv.at[2 * j + 1, c])
            )
            onward[-1].start()
    for copy in mix_copies:
        copy.wait_recv()
    own_wb.wait()
    for copy in beside + onward:
        copy.wait_recv()
    branch = alpha_mix * resid_ref[...].astype(jnp.float32)
    for k in range(n_tp):
        branch = branch + dot(token_rows[k], wb_all[k])
    out_ref[...] = layer_norm(branch, gain_ref[...]).astype(jnp.bfloat16)
    halo_copy.wait_send()
    for copy in stat_copies + mix_copies + cross + beside + onward:
        copy.wait_send()


def expert_kernel(
    n_sp, n_tp, cap, parts,
    normed_ref, ids_ref, wts_ref, eg_hbm, eu_hbm, ed_hbm, sg_hbm, su_hbm, sd_hbm, gain_ref,
    out_ref,
    eg, eu, ed, sg, su, sd, outgoing, arrived, answers, returned, acc, pick, share,
    load_sem, go_send, go_recv, back_send, back_recv,
):
    n = n_sp * n_tp
    s, p = lax.axis_index("sp"), lax.axis_index("tp")
    me = s * n_tp + p
    toks = normed_ref.shape[0]
    per = n // parts
    span = per * cap

    def place(k):
        d = lax.rem(k, n)
        return (d // n_tp, lax.rem(d, n_tp))

    barrier = pltpu.get_barrier_semaphore()

    @pl.loop(1, n)
    def _(o):
        pl.semaphore_signal(barrier, inc=1, device_id=place(me + o), device_id_type=MESH)

    loads = [
        pltpu.make_async_copy(a, b, load_sem.at[i])
        for i, (a, b) in enumerate(
            [(sg_hbm, sg), (su_hbm, su), (sd_hbm, sd), (eg_hbm.at[0], eg), (eu_hbm.at[0], eu), (ed_hbm.at[0], ed)]
        )
    ]
    for load in loads:
        load.start()

    ahead = lax.broadcasted_iota(jnp.int32, (n, toks), 0)
    chosen = jnp.zeros((n, toks), jnp.float32)
    weight = jnp.zeros((n, toks), jnp.float32)
    for k in range(ids_ref.shape[0]):
        rel = ids_ref[k : k + 1, :] - me
        rel = jnp.where(rel < 0, rel + n, rel)
        hit = ahead == rel
        chosen = chosen + jnp.where(hit, 1.0, 0.0)
        weight = weight + jnp.where(hit, wts_ref[k : k + 1, :], 0.0)
    earlier = lax.broadcasted_iota(jnp.int32, (toks, toks), 0) < lax.broadcasted_iota(jnp.int32, (toks, toks), 1)
    rank = dot(chosen.astype(jnp.bfloat16), earlier.astype(jnp.float32).astype(jnp.bfloat16))
    key = jnp.where(chosen > 0.0, rank, -1.0)
    slot = lax.broadcasted_iota(jnp.int32, (n, cap, toks), 1).astype(jnp.float32)
    taken = slot == key[:, None, :]
    pick[...] = jnp.where(taken, 1.0, 0.0).reshape(n * cap, toks).astype(jnp.bfloat16)
    full = jnp.where(taken, weight[:, None, :], 0.0).reshape(n * cap, toks)
    high = full.astype(jnp.bfloat16)
    share[:, 0:toks] = high
    share[:, toks:] = (full - high.astype(jnp.float32)).astype(jnp.bfloat16)

    def chunk(o):
        return pl.ds(pl.multiple_of(o * cap, cap), cap)

    def part(g):
        return pl.ds(pl.multiple_of(g * span, span), span)

    def go(o):
        return pltpu.make_async_remote_copy(
            src_ref=outgoing.at[chunk(o)], dst_ref=arrived.at[chunk(o)],
            send_sem=go_send.at[o], recv_sem=go_recv.at[o],
            device_id=place(me + o), device_id_type=MESH,
        )

    def back(o):
        return pltpu.make_async_remote_copy(
            src_ref=answers.at[chunk(o)], dst_ref=returned.at[chunk(o)],
            send_sem=back_send.at[o], recv_sem=back_recv.at[o],
            device_id=place(me + n - o), device_id_type=MESH,
        )

    def each(g, act):
        @pl.loop(jnp.maximum(g * per, 1), (g + 1) * per)
        def _(o):
            act(o)

    @pl.loop(0, parts)
    def _(g):
        outgoing[part(g), :] = dot(pick[part(g), :], normed_ref[...]).astype(jnp.bfloat16)

    arrived[0:cap, :] = outgoing[0:cap, :]
    pl.semaphore_wait(barrier, n - 1)

    @pl.loop(1, n)
    def _(o):
        go(o).start()

    normed = normed_ref[...]
    for load in loads[:3]:
        load.wait()
    hidden = silu_mul(dot(normed, sg[...]), dot(normed, su[...]))
    acc[...] = alpha_mix * normed.astype(jnp.float32) + dot(hidden, sd[...])
    for load in loads[3:]:
        load.wait()

    @pl.loop(0, parts)
    def _(g):
        each(g, lambda o: go(o).wait_recv())
        tokens = arrived[part(g), :]
        inner = silu_mul(dot(tokens, eg[...]), dot(tokens, eu[...]))
        answers[part(g), :] = dot(inner, ed[...]).astype(jnp.bfloat16)
        each(g, lambda o: back(o).start())

    returned[0:cap, :] = answers[0:cap, :]

    @pl.loop(0, parts)
    def _(g):
        each(g, lambda o: back(o).wait_recv())
        both = lax.dot_general(
            share[part(g), :], returned[part(g), :], (((0,), (0,)), ((), ())),
            preferred_element_type=jnp.float32,
        )
        acc[...] += both[0:toks] + both[toks:]

    out_ref[...] = layer_norm(acc[...], gain_ref[...]).astype(jnp.bfloat16)

    @pl.loop(1, n)
    def _(o):
        go(o).wait_send()
        back(o).wait_send()


def local(
    n_sp, n_tp,
    resid, pool_in, doc_ids, w_group, pool_scale, w_branch, norm_gain, route_ids, route_wts,
    w_exp_gate, w_exp_up, w_exp_down, w_sh_gate, w_sh_up, w_sh_down, final_gain,
):
    toks, width = pool_in.shape
    rows, model = resid.shape
    depth = w_branch.shape[0]
    n = n_sp * n_tp
    cap = max(16, 2 * rows * route_ids.shape[1] // n)
    parts = 4
    ff = w_sh_gate.shape[1]
    vmem, hbm = pl.BlockSpec(memory_space=pltpu.VMEM), pl.BlockSpec(memory_space=pl.ANY)
    dma = pltpu.SemaphoreType.DMA
    bf16, f32 = jnp.bfloat16, jnp.float32
    normed = pl.pallas_call(
        functools.partial(pool_kernel, n_sp, n_tp),
        out_shape=jax.ShapeDtypeStruct((rows, model), bf16),
        in_specs=[vmem] * 5 + [hbm] + [vmem] * 2,
        out_specs=vmem,
        scratch_shapes=[
            pltpu.VMEM((halo + toks, width), bf16),
            pltpu.VMEM((n_sp, 8, width + 128), f32),
            pltpu.VMEM((toks, width), bf16),
            pltpu.VMEM((n_tp, rows, width), bf16),
            pltpu.VMEM((n_tp, depth, model), bf16),
            dma((n_sp,)), dma((n_sp,)), dma, dma, dma((n_tp,)), dma((n_tp,)),
            dma((n_tp, wb_chunks)), dma((n_tp, wb_chunks)), dma((n_tp, wb_chunks)), dma,
        ],
        compiler_params=pltpu.CompilerParams(
            collective_id=0, has_side_effects=True, vmem_limit_bytes=48 << 20
        ),
        name="pool_mixer",
    )(
        pool_in, doc_ids[:, None], doc_ids[None, :], w_group, pool_scale[None, :], w_branch,
        resid, norm_gain[None, :],
    )
    return pl.pallas_call(
        functools.partial(expert_kernel, n_sp, n_tp, cap, parts),
        out_shape=jax.ShapeDtypeStruct((rows, model), bf16),
        in_specs=[vmem] * 3 + [hbm] * 6 + [vmem],
        out_specs=vmem,
        scratch_shapes=[
            pltpu.VMEM((model, ff), bf16), pltpu.VMEM((model, ff), bf16), pltpu.VMEM((ff, model), bf16),
            pltpu.VMEM((model, ff), bf16), pltpu.VMEM((model, ff), bf16), pltpu.VMEM((ff, model), bf16),
            pltpu.VMEM((n * cap, model), bf16), pltpu.VMEM((n * cap, model), bf16),
            pltpu.VMEM((n * cap, model), bf16), pltpu.VMEM((n * cap, model), bf16),
            pltpu.VMEM((rows, model), f32),
            pltpu.VMEM((n * cap, rows), bf16), pltpu.VMEM((n * cap, 2 * rows), bf16),
            dma((6,)), dma((n,)), dma((n,)), dma((n,)), dma((n,)),
        ],
        compiler_params=pltpu.CompilerParams(
            collective_id=1, has_side_effects=True, vmem_limit_bytes=62 << 20
        ),
        name="routed_experts",
    )(
        normed, route_ids.T, route_wts.T, w_exp_gate, w_exp_up, w_exp_down,
        w_sh_gate, w_sh_up, w_sh_down, final_gain[None, :],
    )


def solution(mesh):
    both = P(("sp", "tp"), None)
    stack = P(("sp", "tp"), None, None)
    placed = (
        both, P("sp", "tp"), P("sp"), P(), P(), P("tp", None), P(), both, both,
        stack, stack, stack, P(), P(), P(), P(),
    )
    return jax.shard_map(
        functools.partial(local, mesh.shape["sp"], mesh.shape["tp"]),
        mesh=mesh, in_specs=placed, out_specs=both, check_vma=False,
    )
```

time: 371 us -> 269 us (0.73)
  Pallas kernels: 0 us -> 258 us
  blocking collectives: 132 us -> 0 us
  waiting for transfers between devices: 97.8 us -> 0 us
  local copies, waits for them, and re-layouts: 39.7 us -> 11 us
  matrix products: 26.2 us -> 0 us
  loops' own time: 23.8 us -> 0 us
  other arithmetic: 23.3 us -> 0 us
  between operations: 14.4 us -> 0.05 us
  starting transfers between devices: 12.3 us -> 0 us
    pallas_call x0 -> x2, Pallas kernels: none -> 258 us  [the longest x1 223 us: local(): pl.pallas_call(functools.partial(expert_kernel, n_sp, n_tp, cap, parts),...]
    all_to_all x2 -> x0, waiting for transfers between devices: 97.8 us -> none  [the longest x1 91.8 us: local(): lax.all_to_all(expert_out.reshape(arrived.shape), ('sp', 'tp'), split_axi...]
    all_to_all x1 -> x0, blocking collectives: 96.5 us -> none  [local(): lax.all_to_all(outgoing, ('sp', 'tp'), split_axis=0, concat_axis=0, tiled...]
    dot_general x6 -> x0, matrix products: 26.2 us -> none  [the longest x1 10.1 us: local(): jnp.dot(hidden, w_exp_down[0], preferred_element_type=jnp.float32)]
    another operation x1 -> x0, loops' own time: 23.8 us -> none  [carried_in(): return lax.fori_loop(0, length, lap, start)]
    all_gather x1 -> x0, blocking collectives: 18.7 us -> none  [carried_in(): everything = jax.tree.map(lambda part: lax.all_gather(part, axis), value)]
    unnamed x1 -> x0, blocking collectives: 17.1 us -> none
    gather x3 -> x0, local copies, waits for them, and re-layouts: 16.4 us -> none  [the longest x1 7.96 us: local(): returned[slot_index].astype(jnp.float32)]
  transfers between devices with their start and end apart: 4 -> 0, of which waited for: 2 -> 0; matrix products, arithmetic and copies ran while one was open for 10% -> 0% of each run, Pallas kernels for 0% -> 0%
where the time goes in v1:
time: 269 us
  Pallas kernels  258 us (96%)
  local copies, waits for them, and re-layouts  11 us (4%)
    pallas_call x1, Pallas kernels, local(): pl.pallas_call(functools.partial(expert_kernel, n_sp, n_tp, cap, parts),...  223 us
    pallas_call x1, Pallas kernels, local(): pl.pallas_call(functools.partial(pool_kernel, n_sp, n_tp), out_shape=jax....  34.9 us
    unnamed x13, local copies, waits for them, and re-layouts  7.51 us

profile of v1, /device:TPU:0, one launch (start us, length us, event | category | flops | bytes accessed | tf_op | source)
XLA Modules:
  0.0 268.8 jit_solution(15973685462297441752)
XLA Ops:
  0.0 0.7 broadcast_in_dim.17.scale_ref
  0.7 0.7 broadcast_in_dim.18.gain_ref
  1.4 1.3 broadcast_in_dim.19.gain_ref
  2.7 0.8 copy.17.docc_ref
  3.5 0.0 copy-start.1
  3.5 1.2 copy-done.1
  4.7 0.0 copy-start.2
  4.7 1.0 copy-done.2
  5.8 0.0 copy-start.3
  5.8 0.9 copy-done.3
  6.7 0.0 copy-start.4
  6.7 0.9 copy-done.4
  7.7 0.0 copy-start.5
  7.7 0.7 copy-done.5
  8.3 34.9 %pool_mixer.1.normed_ref = bf16[128,2048]{1,0:T(8,128)(2,1)S(1)} custom-call(bf16[512,256]{1,0:T(8,128)(2,1)S(1)} %copy-done.3, s32[512,1]{1,0:T(8,128)S(1)} %copy.17.docc_ref, s32[1,512]{1,0:T(1,128)S(1)} %bitcast.5, bf16[8,128,128]{2,1,0:T(8,128)(2,1)S(1)} %copy-done.4, bf16[1,1024]{1,0:T(2,128)(2,1)S(1)} %broadcast_in_dim.17.scale_ref, ...), custom_call_target="tpu_custom_call" | custom-call | tf_op jit(solution)/shard_map/pool_mixer/pallas_call | solution.py:320
  43.2 0.0 copy-start
  43.2 0.8 copy-done
  44.0 222.9 %routed_experts.1 = bf16[128,2048]{1,0:T(8,128)(2,1)} custom-call(bf16[128,2048]{1,0:T(8,128)(2,1)} %copy-done, s32[4,128]{1,0:T(4,128)} %bitcast.6, f32[4,128]{1,0:T(4,128)} %bitcast.7, bf16[1,2048,512]{2,1,0:T(8,128)(2,1)} %eg_hbm.1, bf16[1,2048,512]{2,1,0:T(8,128)(2,1)} %eu_hbm.1, bf16[1,512,2048]{2,1,0:T(8,128)(2,1)} %ed_hbm.1, ...), custom_call_target="tpu_custom_call" | custom-call | tf_op jit(solution)/shard_map/routed_experts/pallas_call | solution.py:342
  266.9 1.9 copy.19
Async XLA Ops:
  3.5 1.2 copy-start.1
  4.7 1.0 copy-start.2
  5.8 0.9 copy-start.3
  6.7 0.9 copy-start.4
  7.7 0.7 copy-start.5
  43.2 0.8 copy-start

commit v2 on v1

--- a/solution.py
+++ b/solution.py
@@ -31,8 +31,8 @@
 
 def pool_kernel(
     n_sp, n_tp,
-    pool_ref, docc_ref, docr_ref, wg_ref, scale_ref, wb_ref, resid_ref, gain_ref,
-    out_ref,
+    pool_ref, docc_ref, docr_ref, wg_ref, scale_ref, wb_ref, resid_ref, gain_ref, meta_ref,
+    out_ref, metas_ref,
     ext, stats, mixed, token_rows, wb_all,
     stat_send, stat_recv, halo_send, halo_recv, mix_send, mix_recv,
     wb_send, wb_recv, fw_send, wb_local,
@@ -71,6 +71,7 @@
     sums = dot(jnp.broadcast_to(tail, (8, toks)).astype(jnp.bfloat16), values)
     lane = lax.broadcasted_iota(jnp.int32, (8, 128), 1)
     stats[s, :, 0:width] = sums
+    stats[s, :, width + 128 :] = meta_ref[...]
     stats[s, :, width : width + 128] = jnp.where(lane == 0, last.astype(jnp.float32), tail_count)
 
     halo_copy = pltpu.make_async_remote_copy(
@@ -173,34 +174,31 @@
     for k in range(n_tp):
         branch = branch + dot(token_rows[k], wb_all[k])
     out_ref[...] = layer_norm(branch, gain_ref[...]).astype(jnp.bfloat16)
+    metas_ref[...] = stats[:, :, width + 128 :]
     halo_copy.wait_send()
     for copy in stat_copies + mix_copies + cross + beside + onward:
         copy.wait_send()
 
 
 def expert_kernel(
-    n_sp, n_tp, cap, parts,
-    normed_ref, ids_ref, wts_ref, eg_hbm, eu_hbm, ed_hbm, sg_hbm, su_hbm, sd_hbm, gain_ref,
+    n_sp, n_tp, n_x, cap,
+    normed_ref, metas_ref, eg_hbm, eu_hbm, ed_hbm, sg_hbm, su_hbm, sd_hbm, gain_ref,
     out_ref,
-    eg, eu, ed, sg, su, sd, outgoing, arrived, answers, returned, acc, pick, share,
-    load_sem, go_send, go_recv, back_send, back_recv,
+    eg, eu, ed, sg, su, sd, blocks, outgoing, arrived, returned, column, across, chain, acc, pick, share,
+    load_sem, up_send, down_send, x_send, block_recv, go_send, go_recv, back_send, back_recv,
+    across_send, across_recv, chain_send, chain_recv,
 ):
-    n = n_sp * n_tp
+    n_z = n_sp // n_x
     s, p = lax.axis_index("sp"), lax.axis_index("tp")
-    me = s * n_tp + p
+    z, x = s // n_x, lax.rem(s, n_x)
     toks = normed_ref.shape[0]
-    per = n // parts
-    span = per * cap
-
-    def place(k):
-        d = lax.rem(k, n)
-        return (d // n_tp, lax.rem(d, n_tp))
+    top = metas_ref.shape[1] // 2
 
     barrier = pltpu.get_barrier_semaphore()
-
-    @pl.loop(1, n)
-    def _(o):
-        pl.semaphore_signal(barrier, inc=1, device_id=place(me + o), device_id_type=MESH)
+    for k in range(1, n_sp):
+        pl.semaphore_signal(barrier, inc=1, device_id=(lax.rem(s + k, n_sp), p), device_id_type=MESH)
+    for k in range(1, n_tp):
+        pl.semaphore_signal(barrier, inc=1, device_id=(s, lax.rem(p + k, n_tp)), device_id_type=MESH)
 
     loads = [
         pltpu.make_async_copy(a, b, load_sem.at[i])
@@ -210,96 +208,222 @@
     ]
     for load in loads:
         load.start()
-
-    ahead = lax.broadcasted_iota(jnp.int32, (n, toks), 0)
-    chosen = jnp.zeros((n, toks), jnp.float32)
-    weight = jnp.zeros((n, toks), jnp.float32)
-    for k in range(ids_ref.shape[0]):
-        rel = ids_ref[k : k + 1, :] - me
-        rel = jnp.where(rel < 0, rel + n, rel)
-        hit = ahead == rel
+    blocks[s] = normed_ref[...]
+
+    low = jnp.minimum(z, n_z - 1 - z)
+    rising = jnp.where(z * 2 < n_z, 1, -1)
+    near = [z]
+    for i in range(1, n_z):
+        swing = z - (i + 1) // 2 if i % 2 else z + i // 2
+        near.append(jnp.where(2 * low >= i, swing, z + rising * (i - low)))
+
+    def copy(src, dst, send, recv, where):
+        return pltpu.make_async_remote_copy(
+            src_ref=src, dst_ref=dst, send_sem=send, recv_sem=recv, device_id=where, device_id_type=MESH
+        )
+
+    def up(zb):
+        k = zb * n_x + x
+        return copy(blocks.at[k], blocks.at[k], up_send.at[zb], block_recv.at[k], (jnp.minimum(s + n_x, n_sp - 1), p))
+
+    def down(zb):
+        k = zb * n_x + x
+        return copy(blocks.at[k], blocks.at[k], down_send.at[zb], block_recv.at[k], (jnp.maximum(s - n_x, 0), p))
+
+    def beside(zb, o):
+        k = zb * n_x + x
+        where = (z * n_x + lax.rem(x + o, n_x), p)
+        return copy(blocks.at[k], blocks.at[k], x_send.at[zb, o], block_recv.at[k], where)
+
+    def arrival(k):
+        where = (lax.rem(s + 1, n_sp), p)
+        return copy(blocks.at[k], blocks.at[k], x_send.at[0, 0], block_recv.at[k], where)
+
+    def rises(zb):
+        return (zb <= z) & (z + 1 < n_z)
+
+    def sinks(zb):
+        return (zb >= z) & (z > 0)
+
+    def relay(zb):
+        @pl.when(rises(zb))
+        def _():
+            up(zb).start()
+
+        @pl.when(sinks(zb))
+        def _():
+            down(zb).start()
+
+        for o in range(1, n_x):
+            beside(zb, o).start()
+
+    def seat(j):
+        return pl.ds(j * cap, cap)
+
+    def go(k, j):
+        return copy(
+            outgoing.at[k, seat(j)], arrived.at[k, seat(j)], go_send.at[k, j], go_recv.at[k, j],
+            (s, lax.rem(p + j, n_tp)),
+        )
+
+    def back(k, j):
+        return copy(
+            arrived.at[k, seat(j)], returned.at[k, seat(j)], back_send.at[k, j], back_recv.at[k, j],
+            (s, lax.rem(p + n_tp - j, n_tp)),
+        )
+
+    def send_partial(zb, o):
+        xb = lax.rem(x + o, n_x)
+        k = zb * n_x + xb
+        return copy(
+            blocks.at[k], across.at[zb, o], across_send.at[zb, o], across_recv.at[zb, o], (z * n_x + xb, p)
+        )
+
+    def index(i, o):
+        return near[i] * n_x + lax.rem(x + o, n_x)
+
+    def dispatch(i, o):
+        k = index(i, o)
+        if i or o:
+            arrival(k).wait_recv()
+            if not o:
+                relay(near[i])
+        outgoing[k] = dot(pick[k], blocks[k]).astype(jnp.bfloat16)
+        for j in range(1, n_tp):
+            go(k, j).start()
+        arrived[k, seat(0)] = outgoing[k, seat(0)]
+
+    def experts(i, o):
+        k = index(i, o)
+        for j in range(1, n_tp):
+            go(k, j).wait_recv()
+        tokens = arrived[k]
+        inner = silu_mul(dot(tokens, eg[...]), dot(tokens, eu[...]))
+        arrived[k] = dot(inner, ed[...]).astype(jnp.bfloat16)
+        for j in range(1, n_tp):
+            back(k, j).start()
+        returned[k, seat(0)] = arrived[k, seat(0)]
+
+    def combine(i, o):
+        k = index(i, o)
+        for j in range(1, n_tp):
+            back(k, j).wait_recv()
+        both = lax.dot_general(
+            share[k], returned[k], (((0,), (0,)), ((), ())), preferred_element_type=jnp.float32
+        )
+        partial = both[0:toks] + both[toks:]
+        if o:
+            blocks[k] = partial.astype(jnp.bfloat16)
+            send_partial(near[i], o).start()
+        else:
+            column[near[i]] = partial
+
+    pl.semaphore_wait(barrier, n_sp + n_tp - 2)
+    relay(z)
+
+    pad = -(-n_tp // 8) * 8
+    expert = s * n_tp + lax.rem(p + lax.broadcasted_iota(jnp.int32, (n_sp, pad, toks), 1), n_tp)
+    expert = expert.astype(jnp.float32)
+    chosen = jnp.zeros((n_sp, pad, toks), jnp.float32)
+    weight = jnp.zeros((n_sp, pad, toks), jnp.float32)
+    for a in range(top):
+        hit = metas_ref[:, a : a + 1, :] == expert
         chosen = chosen + jnp.where(hit, 1.0, 0.0)
-        weight = weight + jnp.where(hit, wts_ref[k : k + 1, :], 0.0)
+        weight = weight + jnp.where(hit, metas_ref[:, top + a : top + a + 1, :], 0.0)
     earlier = lax.broadcasted_iota(jnp.int32, (toks, toks), 0) < lax.broadcasted_iota(jnp.int32, (toks, toks), 1)
-    rank = dot(chosen.astype(jnp.bfloat16), earlier.astype(jnp.float32).astype(jnp.bfloat16))
+    rank = dot(
+        chosen.reshape(n_sp * pad, toks).astype(jnp.bfloat16), earlier.astype(jnp.float32).astype(jnp.bfloat16)
+    ).reshape(n_sp, pad, toks)
     key = jnp.where(chosen > 0.0, rank, -1.0)
-    slot = lax.broadcasted_iota(jnp.int32, (n, cap, toks), 1).astype(jnp.float32)
-    taken = slot == key[:, None, :]
-    pick[...] = jnp.where(taken, 1.0, 0.0).reshape(n * cap, toks).astype(jnp.bfloat16)
-    full = jnp.where(taken, weight[:, None, :], 0.0).reshape(n * cap, toks)
-    high = full.astype(jnp.bfloat16)
-    share[:, 0:toks] = high
-    share[:, toks:] = (full - high.astype(jnp.float32)).astype(jnp.bfloat16)
-
-    def chunk(o):
-        return pl.ds(pl.multiple_of(o * cap, cap), cap)
-
-    def part(g):
-        return pl.ds(pl.multiple_of(g * span, span), span)
-
-    def go(o):
-        return pltpu.make_async_remote_copy(
-            src_ref=outgoing.at[chunk(o)], dst_ref=arrived.at[chunk(o)],
-            send_sem=go_send.at[o], recv_sem=go_recv.at[o],
-            device_id=place(me + o), device_id_type=MESH,
-        )
-
-    def back(o):
-        return pltpu.make_async_remote_copy(
-            src_ref=answers.at[chunk(o)], dst_ref=returned.at[chunk(o)],
-            send_sem=back_send.at[o], recv_sem=back_recv.at[o],
-            device_id=place(me + n - o), device_id_type=MESH,
-        )
-
-    def each(g, act):
-        @pl.loop(jnp.maximum(g * per, 1), (g + 1) * per)
-        def _(o):
-            act(o)
-
-    @pl.loop(0, parts)
-    def _(g):
-        outgoing[part(g), :] = dot(pick[part(g), :], normed_ref[...]).astype(jnp.bfloat16)
-
-    arrived[0:cap, :] = outgoing[0:cap, :]
-    pl.semaphore_wait(barrier, n - 1)
-
-    @pl.loop(1, n)
-    def _(o):
-        go(o).start()
-
-    normed = normed_ref[...]
-    for load in loads[:3]:
-        load.wait()
-    hidden = silu_mul(dot(normed, sg[...]), dot(normed, su[...]))
-    acc[...] = alpha_mix * normed.astype(jnp.float32) + dot(hidden, sd[...])
-    for load in loads[3:]:
-        load.wait()
-
-    @pl.loop(0, parts)
-    def _(g):
-        each(g, lambda o: go(o).wait_recv())
-        tokens = arrived[part(g), :]
-        inner = silu_mul(dot(tokens, eg[...]), dot(tokens, eu[...]))
-        answers[part(g), :] = dot(inner, ed[...]).astype(jnp.bfloat16)
-        each(g, lambda o: back(o).start())
-
-    returned[0:cap, :] = answers[0:cap, :]
-
-    @pl.loop(0, parts)
-    def _(g):
-        each(g, lambda o: back(o).wait_recv())
-        both = lax.dot_general(
-            share[part(g), :], returned[part(g), :], (((0,), (0,)), ((), ())),
-            preferred_element_type=jnp.float32,
-        )
-        acc[...] += both[0:toks] + both[toks:]
-
-    out_ref[...] = layer_norm(acc[...], gain_ref[...]).astype(jnp.bfloat16)
-
-    @pl.loop(1, n)
-    def _(o):
-        go(o).wait_send()
-        back(o).wait_send()
+    slot = lax.broadcasted_iota(jnp.int32, (n_sp, cap, toks), 1).astype(jnp.float32)
+    for j in range(n_tp):
+        taken = slot == key[:, j : j + 1, :]
+        pick[:, seat(j), :] = jnp.where(taken, 1.0, 0.0).astype(jnp.bfloat16)
+        full = jnp.where(taken, weight[:, j : j + 1, :], 0.0)
+        high = full.astype(jnp.bfloat16)
+        share[:, seat(j), 0:toks] = high
+        share[:, seat(j), toks:] = (full - high.astype(jnp.float32)).astype(jnp.bfloat16)
+
+    order = [(0, 0)]
+    for i in range(1, n_z):
+        order += [(i, 0)] + [(i - 1, o) for o in range(1, n_x)]
+    order += [(n_z - 1, o) for o in range(1, n_x)]
+    for at in range(len(order) + 3):
+        if at < len(order):
+            dispatch(*order[at])
+        if at == 0:
+            for load in loads[:3]:
+                load.wait()
+            hidden = silu_mul(dot(normed_ref[...], sg[...]), dot(normed_ref[...], su[...]))
+            acc[...] = alpha_mix * normed_ref[...].astype(jnp.float32) + dot(hidden, sd[...])
+            for load in loads[3:]:
+                load.wait()
+        if 0 <= at - 1 < len(order):
+            experts(*order[at - 1])
+        if 0 <= at - 3 < len(order):
+            combine(*order[at - 3])
+
+    for zb in range(n_z):
+        @pl.when(rises(zb))
+        def _():
+            up(zb).wait_send()
+
+        @pl.when(sinks(zb))
+        def _():
+            down(zb).wait_send()
+
+        for o in range(1, n_x):
+            beside(zb, o).wait_send()
+
+    def column_sum(zb):
+        total = column[zb]
+        for o in range(1, n_x):
+            send_partial(zb, o).wait_recv()
+            total = total + across[zb, o].astype(jnp.float32)
+        column[zb] = total
+
+    def link(side, zb):
+        where = s + n_x if side == 0 else s - n_x
+        where = jnp.maximum(jnp.minimum(where, n_sp - 1), 0)
+        return copy(
+            blocks.at[zb * n_x + x], chain.at[side, zb], chain_send.at[zb], chain_recv.at[side, zb], (where, p)
+        )
+
+    def take(side, zb, holds):
+        @pl.when(holds)
+        def _():
+            link(side, zb).wait_recv()
+            column[zb] += chain[side, zb].astype(jnp.float32)
+
+    for i in range(n_z - 1, 0, -1):
+        zb = near[i]
+        column_sum(zb)
+        take(0, zb, (zb > z) & (z > 0))
+        take(1, zb, (zb < z) & (z + 1 < n_z))
+        blocks[zb * n_x + x] = column[zb].astype(jnp.bfloat16)
+
+        @pl.when(zb > z)
+        def _():
+            link(0, zb).start()
+
+        @pl.when(zb < z)
+        def _():
+            link(1, zb).start()
+
+    column_sum(z)
+    take(0, z, z > 0)
+    take(1, z, z + 1 < n_z)
+    out_ref[...] = layer_norm(acc[...] + column[z], gain_ref[...]).astype(jnp.bfloat16)
+
+    for i in range(1, n_z):
+        link(0, near[i]).wait_send()
+    for k in range(n_sp):
+        for j in range(1, n_tp):
+            go(k, j).wait_send()
+            back(k, j).wait_send()
+    for zb in range(n_z):
+        for o in range(1, n_x):
+            send_partial(zb, o).wait_send()
 
 
 def local(
@@ -310,21 +434,25 @@
     toks, width = pool_in.shape
     rows, model = resid.shape
     depth = w_branch.shape[0]
-    n = n_sp * n_tp
-    cap = max(16, 2 * rows * route_ids.shape[1] // n)
-    parts = 4
+    cap = 2 * rows * route_ids.shape[1] // (n_sp * n_tp)
+    n_x = max(k for k in range(1, n_sp + 1) if n_sp % k == 0 and k * k <= n_sp)
+    n_z = n_sp // n_x
     ff = w_sh_gate.shape[1]
+    meta = jnp.concatenate([route_ids.astype(jnp.float32), route_wts], axis=1).T
     vmem, hbm = pl.BlockSpec(memory_space=pltpu.VMEM), pl.BlockSpec(memory_space=pl.ANY)
     dma = pltpu.SemaphoreType.DMA
     bf16, f32 = jnp.bfloat16, jnp.float32
-    normed = pl.pallas_call(
+    normed, metas = pl.pallas_call(
         functools.partial(pool_kernel, n_sp, n_tp),
-        out_shape=jax.ShapeDtypeStruct((rows, model), bf16),
-        in_specs=[vmem] * 5 + [hbm] + [vmem] * 2,
-        out_specs=vmem,
+        out_shape=(
+            jax.ShapeDtypeStruct((rows, model), bf16),
+            jax.ShapeDtypeStruct((n_sp, meta.shape[0], rows), f32),
+        ),
+        in_specs=[vmem] * 5 + [hbm] + [vmem] * 3,
+        out_specs=(vmem, vmem),
         scratch_shapes=[
             pltpu.VMEM((halo + toks, width), bf16),
-            pltpu.VMEM((n_sp, 8, width + 128), f32),
+            pltpu.VMEM((n_sp, 8, width + 128 + rows), f32),
             pltpu.VMEM((toks, width), bf16),
             pltpu.VMEM((n_tp, rows, width), bf16),
             pltpu.VMEM((n_tp, depth, model), bf16),
@@ -337,28 +465,35 @@
         name="pool_mixer",
     )(
         pool_in, doc_ids[:, None], doc_ids[None, :], w_group, pool_scale[None, :], w_branch,
-        resid, norm_gain[None, :],
+        resid, norm_gain[None, :], meta,
     )
+    seats = pltpu.VMEM((n_sp, n_tp * cap, model), bf16)
+    block = (rows, model)
     return pl.pallas_call(
-        functools.partial(expert_kernel, n_sp, n_tp, cap, parts),
-        out_shape=jax.ShapeDtypeStruct((rows, model), bf16),
-        in_specs=[vmem] * 3 + [hbm] * 6 + [vmem],
+        functools.partial(expert_kernel, n_sp, n_tp, n_x, cap),
+        out_shape=jax.ShapeDtypeStruct(block, bf16),
+        in_specs=[vmem] * 2 + [hbm] * 6 + [vmem],
         out_specs=vmem,
         scratch_shapes=[
             pltpu.VMEM((model, ff), bf16), pltpu.VMEM((model, ff), bf16), pltpu.VMEM((ff, model), bf16),
             pltpu.VMEM((model, ff), bf16), pltpu.VMEM((model, ff), bf16), pltpu.VMEM((ff, model), bf16),
-            pltpu.VMEM((n * cap, model), bf16), pltpu.VMEM((n * cap, model), bf16),
-            pltpu.VMEM((n * cap, model), bf16), pltpu.VMEM((n * cap, model), bf16),
-            pltpu.VMEM((rows, model), f32),
-            pltpu.VMEM((n * cap, rows), bf16), pltpu.VMEM((n * cap, 2 * rows), bf16),
-            dma((6,)), dma((n,)), dma((n,)), dma((n,)), dma((n,)),
+            pltpu.VMEM((n_sp, *block), bf16),
+            seats, seats, seats,
+            pltpu.VMEM((n_z, *block), f32),
+            pltpu.VMEM((n_z, n_x, *block), bf16),
+            pltpu.VMEM((2, n_z, *block), bf16),
+            pltpu.VMEM(block, f32),
+            pltpu.VMEM((n_sp, n_tp * cap, rows), bf16), pltpu.VMEM((n_sp, n_tp * cap, 2 * rows), bf16),
+            dma((6,)), dma((n_z,)), dma((n_z,)), dma((n_z, n_x)), dma((n_sp,)),
+            dma((n_sp, n_tp)), dma((n_sp, n_tp)), dma((n_sp, n_tp)), dma((n_sp, n_tp)),
+            dma((n_z, n_x)), dma((n_z, n_x)), dma((n_z,)), dma((2, n_z)),
         ],
         compiler_params=pltpu.CompilerParams(
             collective_id=1, has_side_effects=True, vmem_limit_bytes=62 << 20
         ),
         name="routed_experts",
     )(
-        normed, route_ids.T, route_wts.T, w_exp_gate, w_exp_up, w_exp_down,
+        normed, metas, w_exp_gate, w_exp_up, w_exp_down,
         w_sh_gate, w_sh_up, w_sh_down, final_gain[None, :],
     )
 

time: 269 us -> 204 us (0.76)
  Pallas kernels: 258 us -> 191 us
    pallas_call x2, Pallas kernels: 258 us -> 191 us  [the longest x1 156 us: local(): pl.pallas_call(functools.partial(expert_kernel, n_sp, n_tp, n_x, cap), ou...]
    unnamed x13 -> x15, local copies, waits for them, and re-layouts: 7.51 us -> 8.11 us
where the time goes in v2:
time: 204 us
  Pallas kernels  191 us (94%)
  local copies, waits for them, and re-layouts  11.6 us (6%)
    pallas_call x1, Pallas kernels, local(): pl.pallas_call(functools.partial(expert_kernel, n_sp, n_tp, n_x, cap), ou...  156 us
    pallas_call x1, Pallas kernels, local(): pl.pallas_call(functools.partial(pool_kernel, n_sp, n_tp), out_shape=(jax...  34.8 us
    unnamed x15, local copies, waits for them, and re-layouts  8.11 us

profile of v2, /device:TPU:0, one launch (start us, length us, event | category | flops | bytes accessed | tf_op | source)
XLA Modules:
  0.0 203.6 jit_solution(12271960080749079182)
XLA Ops:
  0.0 0.7 convert_element_type.3
  0.7 0.7 maximum_bitcast_fusion.meta_ref
  1.4 0.7 broadcast_in_dim.17.scale_ref
  2.1 0.7 broadcast_in_dim.18.gain_ref
  2.8 1.3 broadcast_in_dim.19.gain_ref
  4.0 0.8 copy.17.docc_ref
  4.9 0.0 copy-start
  4.9 1.2 copy-done
  6.1 0.0 copy-start.2
  6.1 1.0 copy-done.2
  7.1 0.0 copy-start.3
  7.1 0.9 copy-done.3
  8.1 0.0 copy-start.4
  8.1 0.9 copy-done.4
  9.0 0.0 copy-start.6
  9.0 0.7 copy-done.6
  9.7 34.8 %pool_mixer.1 = (bf16[128,2048]{1,0:T(8,128)(2,1)S(1)}, f32[8,8,128]{2,1,0:T(8,128)S(1)}) custom-call(bf16[512,256]{1,0:T(8,128)(2,1)S(1)} %copy-done.3, s32[512,1]{1,0:T(8,128)S(1)} %copy.17.docc_ref, s32[1,512]{1,0:T(1,128)S(1)} %bitcast.5, bf16[8,128,128]{2,1,0:T(8,128)(2,1)S(1)} %copy-done.4, bf16[1,1024]{1,0:T(2,128)(2,1)S(1)} %broadcast_in_dim.17.scale_ref, ...), custom_call_target="tpu_custom_call" | custom-call | tf_op jit(solution)/shard_map/pool_mixer/pallas_call | solution.py:445
  44.6 0.0 copy-start.1
  44.6 0.8 copy-done.1
  45.4 0.0 copy-start.5
  45.4 0.6 copy-done.5
  46.0 155.8 %routed_experts.1 = bf16[128,2048]{1,0:T(8,128)(2,1)} custom-call(bf16[128,2048]{1,0:T(8,128)(2,1)} %copy-done.1, f32[8,8,128]{2,1,0:T(8,128)} %copy-done.5, bf16[1,2048,512]{2,1,0:T(8,128)(2,1)} %eg_hbm.1, bf16[1,2048,512]{2,1,0:T(8,128)(2,1)} %eu_hbm.1, bf16[1,512,2048]{2,1,0:T(8,128)(2,1)} %ed_hbm.1, bf16[2048,512]{1,0:T(8,128)(2,1)} %sg_hbm.1, ...), custom_call_target="tpu_custom_call" | custom-call | tf_op jit(solution)/shard_map/routed_experts/pallas_call | solution.py:472
  201.8 1.9 copy.19
Async XLA Ops:
  4.9 1.2 copy-start
  6.1 1.0 copy-start.2
  7.1 0.9 copy-start.3
  8.1 0.9 copy-start.4
  9.0 0.7 copy-start.6
  44.6 0.8 copy-start.1
  45.4 0.6 copy-start.5
